TPU v7x, 256 devices: a whole 4x4x8 slice. The times are simulated.
256 devices in a mesh: ep: 64 (over z, y, core), tp: 4 (over x).
Axes of the slice: x: 4, y: 4, z: 8, core: 2. Of those that a mesh axis runs over, the one named last changes fastest.
Arguments:
- cell_query_rows: bfloat16 [16384, 2048], P('ep', 'tp'), may hold values from -6 to 6
- cell_key_rows: bfloat16 [16384, 2048], P('ep', 'tp'), may hold values from -6 to 6
- cell_value_rows: bfloat16 [16384, 2048], P('ep', 'tp'), may hold values from -6 to 6
- output_gate_logits: bfloat16 [16384, 2048], P('ep', 'tp'), may hold values from -8 to 8
- log_input_gate: float32 [8, 16384], P('tp', 'ep'), may hold values from -4 to 110
- forget_gate_logits: float32 [8, 16384], P('tp', 'ep'), may hold values from -1 to 25
- extra_log_forget: float32 [8, 16384], P('tp', 'ep'), may hold values from -0.7 to 0
- cell_output_scale: float32 [2048], P('tp'), may hold values from 0.1 to 1.9
- tokens_into_experts: bfloat16 [32768, 2048], P(('ep', 'tp')), may hold values from -6 to 6
- expert_norm_scale: float32 [2048], replicated, may hold values from 0.1 to 1.9
- token_expert_index: int32 [32768, 2], P(('ep', 'tp')), may hold values from 0 to 63, all different within a row; in each aligned block of 128 rows (0 to 127, 128 to 255, ...) at most 5 rows name the same one
- chosen_expert_weight: float32 [32768, 2], P(('ep', 'tp')), may hold values from 0.3 to 3
- expert_gate_weight: bfloat16 [64, 2048, 3584], P('ep', None, 'tp'), may hold values from -0.125 to 0.125
- expert_up_weight: bfloat16 [64, 2048, 3584], P('ep', None, 'tp'), may hold values from -0.125 to 0.125
- expert_down_weight: bfloat16 [64, 3584, 2048], P('ep', 'tp'), may hold values from -0.09375 to 0.09375
Outputs:
- gated_head_output: bfloat16 [16384, 2048], P('ep', 'tp')
- expert_output: bfloat16 [32768, 2048], P(('ep', 'tp'))
Inputs may be any that keep to these rules, and one draw needn't show every extreme that they name: `token_expert_index`: each row names 2 different experts. Among the rows of one device (aligned blocks of 128 rows) no expert is named by more than 5 rows, and in every draw some expert is named by exactly 5 rows of some device.
All inputs are finite; a program needn't handle non-finite values.
Results may differ from a plain program's by a relative error of at most 0.012.
Values may be sent and summed in bfloat16 or wider, within the bound.
No kernel may reach another device: no remote copies, remote signals or barrier semaphores. Data moves between devices by JAX's collectives and lax.ppermute only.
A program may use at most 128 MiB of HBM per device.

v0:
```python
import jax
import jax.numpy as jnp
from jax import lax
from jax.sharding import Mesh
from jax.sharding import PartitionSpec as P

HEAD_DIM = 256
BLOCK = 64
TOPK = 2
EP = ("ep_0", "ep_1", "ep_2")
EP_TP = ("ep_0", "ep_1", "ep_2", "tp")
EPSILON = 1e-06
PRECISE = lax.Precision.HIGHEST


def nothing_yet(x, identity):
    return jax.tree.map(
        lambda part, zero: jnp.zeros_like(part) + jnp.asarray(zero, part.dtype), x, identity
    )


def collected_together(x, axis):
    leaves = jax.tree.leaves(x)
    turns = sorted(range(len(leaves)), key=lambda k: -leaves[k].size)
    width = (1, *leaves[turns[0]].shape)[-1]
    lines = [
        jnp.pad(leaves[k].reshape(-1), (0, -leaves[k].size % width)).reshape(-1, width)
        for k in turns
    ]
    both, at, found = (lax.all_gather(jnp.concatenate(lines), axis), 0, {})
    for k, line in zip(turns, lines):
        share = both[:, at : at + len(line)].reshape(len(both), -1)
        found[k] = share[:, : leaves[k].size].reshape(-1, *leaves[k].shape)
        at += len(line)
    numbers = iter(range(len(leaves)))
    return jax.tree.map(lambda _: found[next(numbers)], x)


def entering(x, axes, combine, identity):
    before = start = nothing_yet(x, identity)
    so_far = x
    for axis in reversed(axes):
        size, here = (lax.axis_size(axis), lax.axis_index(axis))
        pieces = collected_together(so_far, axis)
        inside, so_far = (start, start)
        for k in range(size):
            passed = k < here
            so_far = combine(so_far, jax.tree.map(lambda part: part[k], pieces))
            inside = jax.tree.map(lambda new, old: jnp.where(passed, new, old), so_far, inside)
        before = combine(inside, before)
    return before


def split_up(x, dim, size):
    before, after = (x.shape[:dim], x.shape[dim + 1 :])
    return jnp.moveaxis(x.reshape(*before, size, -1, *after), dim, 0)


def sum_at_owner(x, axis, dim):
    size = lax.axis_size(axis)
    blocks = lax.all_to_all(split_up(x, dim, size), axis, 0, 0, tiled=True)
    return jnp.sum(blocks.astype(jnp.float32), axis=0)


def combine(earlier, later):
    cell_early, norm_early, stab_early, total_early = earlier
    cell_late, norm_late, stab_late, total_late = later
    stabilizer = jnp.maximum(total_late + stab_early, stab_late)
    keep_factor = jnp.exp(total_late + stab_early - stabilizer)
    take_factor = jnp.exp(stab_late - stabilizer)
    cell_state = (
        keep_factor[..., None, None] * cell_early + take_factor[..., None, None] * cell_late
    )
    norm_state = keep_factor[..., None] * norm_early + take_factor[..., None] * norm_late
    return (cell_state, norm_state, stabilizer, total_early + total_late)


def mix_heads(
    cell_query_rows,
    cell_key_rows,
    cell_value_rows,
    output_gate_logits,
    log_input_gate,
    forget_gate_logits,
    extra_log_forget,
    cell_output_scale,
):
    n_tok, row_width = cell_query_rows.shape
    head_count = row_width // HEAD_DIM
    block_count = n_tok // BLOCK
    key_scale = HEAD_DIM ** (-0.5)
    block_shape = (block_count, BLOCK, head_count, HEAD_DIM)
    query_blocks = cell_query_rows.reshape(block_shape)
    key_blocks = cell_key_rows.reshape(block_shape)
    value_blocks = cell_value_rows.reshape(block_shape)
    gate_input = log_input_gate.reshape(head_count, block_count, BLOCK)
    forget_gate_value = (jax.nn.log_sigmoid(forget_gate_logits) + extra_log_forget).reshape(
        head_count, block_count, BLOCK
    )
    cumulative = jnp.cumsum(forget_gate_value, axis=-1)
    block_last = cumulative[..., -1]
    growth = block_last[..., None] - cumulative + gate_input
    block_top = jnp.max(growth, axis=-1)
    shares = jnp.exp(growth - block_top[..., None])
    key_float = key_blocks.astype(jnp.float32) * key_scale
    value_weighted = value_blocks.astype(jnp.float32) * shares.transpose(1, 2, 0)[..., None]
    cell_terms = jnp.einsum("bshv,bshk->bhvk", value_weighted, key_float, precision=PRECISE)
    norm_terms = jnp.einsum("hbs,bshk->bhk", shares, key_float, precision=PRECISE)
    block_terms = (cell_terms, norm_terms, block_top.T, block_last.T)
    identity_state = (
        jnp.zeros((head_count, HEAD_DIM, HEAD_DIM), jnp.float32),
        jnp.zeros((head_count, HEAD_DIM), jnp.float32),
        jnp.full((head_count,), -1e30, jnp.float32),
        jnp.zeros((head_count,), jnp.float32),
    )

    def fold_step(running, block_term):
        return (combine(running, block_term), running)

    device_total, before = lax.scan(fold_step, identity_state, block_terms)
    prior_state = entering(device_total, EP, combine, identity_state)
    zero_state = (
        jnp.zeros((head_count, HEAD_DIM, HEAD_DIM), jnp.float32),
        jnp.zeros((head_count, HEAD_DIM), jnp.float32),
        jnp.zeros((head_count,), jnp.float32),
        jnp.zeros((head_count,), jnp.float32),
    )
    start_state = combine(zero_state, prior_state)
    cell_state, norm_state, stabilizer, _ = combine(start_state, before)
    inter_log = cumulative + stabilizer.T[:, :, None]
    causal = jnp.tril(jnp.ones((BLOCK, BLOCK), dtype=bool))
    spread = jnp.where(
        causal,
        cumulative[..., :, None] - cumulative[..., None, :] + gate_input[..., None, :],
        -jnp.inf,
    )
    row_top = jnp.maximum(inter_log, jnp.max(spread, axis=-1))
    intra_weight = jnp.exp(spread - row_top[..., None])
    inter_weight = jnp.exp(inter_log - row_top)
    scores = (
        jnp.einsum("bthd,bshd->hbts", query_blocks, key_blocks, preferred_element_type=jnp.float32)
        * key_scale
        * intra_weight
    )
    weights = scores.astype(jnp.bfloat16)
    numerator = jnp.einsum(
        "hbts,bshd->hbtd", weights, value_blocks, preferred_element_type=jnp.float32
    )
    query_float = query_blocks.astype(jnp.float32)
    numerator = numerator + inter_weight[..., None] * jnp.einsum(
        "bhvk,bthk->hbtv", cell_state, query_float, precision=PRECISE
    )
    denominator = jnp.sum(scores, axis=-1) + inter_weight * jnp.einsum(
        "bhk,bthk->hbt", norm_state, query_float, precision=PRECISE
    )
    cell_out = numerator / jnp.maximum(jnp.abs(denominator), 1.0)[..., None]
    cell_out = cell_out.transpose(1, 2, 0, 3).reshape(n_tok, row_width)
    return (
        cell_out * cell_output_scale * jax.nn.sigmoid(output_gate_logits.astype(jnp.float32))
    ).astype(jnp.bfloat16)


def slot_tables(ids, experts, capacity):
    flat_ids = ids.reshape(-1)
    onehot = (flat_ids[:, None] == jnp.arange(experts, dtype=jnp.int32)[None, :]).astype(jnp.int32)
    earlier = jnp.cumsum(onehot, axis=0) - onehot
    rank_in = jnp.sum(earlier * onehot, axis=1)
    slot_index = flat_ids * capacity + rank_in
    token_of = jnp.arange(flat_ids.shape[0], dtype=jnp.int32) // ids.shape[1]
    slot_hit = slot_index[:, None] == jnp.arange(experts * capacity, dtype=jnp.int32)[None, :]
    slot_owner = jnp.sum(jnp.where(slot_hit, token_of[:, None] + 1, 0), axis=0)
    return (slot_owner, slot_index.reshape(ids.shape))


def local(
    cell_query_rows,
    cell_key_rows,
    cell_value_rows,
    output_gate_logits,
    log_input_gate,
    forget_gate_logits,
    extra_log_forget,
    cell_output_scale,
    tokens_into_experts,
    expert_norm_scale,
    token_expert_index,
    chosen_expert_weight,
    expert_gate_weight,
    expert_up_weight,
    expert_down_weight,
):
    gated_head_output = mix_heads(
        cell_query_rows,
        cell_key_rows,
        cell_value_rows,
        output_gate_logits,
        log_input_gate,
        forget_gate_logits,
        extra_log_forget,
        cell_output_scale,
    )
    ep_count = lax.axis_size(EP)
    n_tok = tokens_into_experts.shape[0]
    experts = ep_count * expert_gate_weight.shape[0]
    capacity = n_tok * TOPK * 5 // (4 * experts)
    input_float = tokens_into_experts.astype(jnp.float32)
    normed = (
        input_float
        * lax.rsqrt(jnp.mean(input_float * input_float, axis=-1, keepdims=True) + EPSILON)
        * expert_norm_scale
    ).astype(jnp.bfloat16)
    gate_matrix = expert_gate_weight[0]
    up_matrix = expert_up_weight[0]
    down_matrix = expert_down_weight[0]
    slot_owner, slot_index = slot_tables(token_expert_index, experts, capacity)
    sendbuf = jnp.where(
        (slot_owner > 0)[:, None],
        normed[jnp.maximum(slot_owner - 1, 0)],
        jnp.zeros((), jnp.bfloat16),
    )
    arrived = lax.all_to_all(sendbuf, EP, split_axis=0, concat_axis=0, tiled=True)
    routed_rows = lax.all_gather(arrived, "tp", axis=0, tiled=True)
    gate_out = jnp.dot(routed_rows, gate_matrix, preferred_element_type=jnp.float32)
    up_out = jnp.dot(routed_rows, up_matrix, preferred_element_type=jnp.float32)
    hidden = (jax.nn.silu(gate_out) * up_out).astype(jnp.bfloat16)
    summed = sum_at_owner(
        jnp.dot(hidden, down_matrix, preferred_element_type=jnp.float32).astype(jnp.bfloat16),
        "tp",
        0,
    ).astype(jnp.bfloat16)
    returned = lax.all_to_all(summed, EP, split_axis=0, concat_axis=0, tiled=True)
    picked = returned[slot_index]
    expert_output = jnp.sum(
        chosen_expert_weight[..., None] * picked.astype(jnp.float32), axis=1
    ).astype(jnp.bfloat16)
    return (gated_head_output, expert_output)


def solution(mesh):
    finer = Mesh(mesh.devices.reshape(8, 4, 2, mesh.shape["tp"]), ("ep_0", "ep_1", "ep_2", "tp"))
    placed = (
        P(EP, "tp"),
        P(EP, "tp"),
        P(EP, "tp"),
        P(EP, "tp"),
        P("tp", EP),
        P("tp", EP),
        P("tp", EP),
        P("tp"),
        P(EP_TP, None),
        P(),
        P(EP_TP, None),
        P(EP_TP, None),
        P(EP, None, "tp"),
        P(EP, None, "tp"),
        P(EP, "tp", None),
    )
    return jax.shard_map(
        local, mesh=finer, in_specs=placed, out_specs=(P(EP, "tp"), P(EP_TP, None)), check_vma=False
    )
```

profile of v0, /device:TPU:8, one launch (start us, length us, event | category | flops | bytes accessed | tf_op | source)
XLA Modules:
  0.0 352.7 jit_solution(4525034145210452684)
XLA Ops:
  12.4 2.0 fusion.38
  14.4 17.1 %while.25 = (s32[]{:T(128)}, f32[2,256,256]{2,1,0:T(8,128)S(1)}, f32[2,256]{1,0:T(2,128)S(1)}, f32[2]{0:T(128)S(1)}, f32[2]{0:T(128)S(1)}, /*index=5*/f32[4,2,25...) while((s32[]{:T(128)}, f32[2,256,256]{2,1,0:T(8,128)S(1)}, ...), condition=%wide.region_3.4_spmd.clone, body=%wide.region_2.3_spmd.clone.sunk | while | flops 657939 | bytes 2632044 | solution.py:120
  34.4 15.4 %all-gather.13.cloned.1.call-done = f32[2,516,256]{2,1,0:T(8,128)} async-done(((f32[1,516,256]{2,1,0:T(8,128)}), f32[2,516,256]{2,1,0:T(8,128)}) %all-gather.13.cloned.1.call-update) | async-done | bytes 1056784 | tf_op jit(solution)/shard_map/all_gather | solution.py:30
  52.0 1.5 fusion.34
  54.5 2.4 gather_fusion
  58.0 61.6 %all_to_all.26 = bf16[64,5,2048]{2,1,0:T(8,128)(2,1)S(1)} all-to-all(bf16[64,5,2048]{2,1,0:T(8,128)(2,1)S(1)} %broadcast_select_fusion.3), channel_id=1, replica_groups=mesh['ep_0'=8,'ep_1'=4,'ep_2'=2,'tp'=4] {'ep_0','ep_1','ep_2'}, dimensions={0} | all-to-all | bytes 2621440 | tf_op jit(solution)/shard_map/all_to_all | solution.py:221
  123.9 2.0 fusion.27
  126.8 49.9 %all-gather.11.cloned.1.call-done = bf16[1280,2048]{1,0:T(8,128)(2,1)} async-done(((bf16[320,2048]{1,0:T(8,128)(2,1)}), bf16[1280,2048]{1,0:T(8,128)(2,1)}) %all-gather.11.cloned.1.call-update) | async-done | bytes 5242896 | tf_op jit(solution)/shard_map/all_gather | solution.py:222
  176.7 9.9 %fusion.11 = f32[1280,896]{1,0:T(8,128)} fusion(bf16[1280,2048]{1,0:T(8,128)(2,1)} %all-gather.11.cloned.1.call-done, bf16[1,2048,896]{2,1,0:T(8,128)(2,1)} %param.29), kind=kOutput, calls=%fused_computation.26 | convolution fusion | flops 4697620480 | bytes 13500416 | tf_op jit(solution)/shard_map/dot_general | solution.py:223
  186.7 17.7 %convolution_convert_fusion = bf16[1280,2048]{1,0:T(8,128)(2,1)} fusion(bf16[1,896,2048]{2,1,0:T(8,128)(2,1)} %param.31, f32[1280,896]{1,0:T(8,128)} %fusion.11, bf16[1280,2048]{1,0:T(8,128)(2,1)} %all-gather.11.cloned.1.call-done, bf16[1,2048,896]{2,1,0:T(8,128)(2,1)} %param.30), kind=kOutput, calls=%fused_computation.22 | convolution fusion | flops 9404743680 | bytes 22413312 | tf_op jit(solution)/shard_map/dot_general | solution.py:227
  204.4 5.2 %all-to-all-start.1 = ((bf16[4,320,2048]{2,1,0:T(8,128)(2,1)}), bf16[4,320,2048]{2,1,0:T(8,128)(2,1)}, u32[]{:S(2)}, u32[]{:S(2)}) async-start(bf16[4,320,2048]{2,1,0:T(8,128)(2,1)} %bitcast.529), calls=%async_computation.1 | async-start | bytes 10485760 | tf_op jit(solution)/shard_map/all_to_all | solution.py:61
  213.9 1.4 fusion.132
  215.3 19.0 %all-gather.17.cloned.1.call-done = f32[8,516,256]{2,1,0:T(8,128)} async-done(((f32[1,516,256]{2,1,0:T(8,128)}), f32[8,516,256]{2,1,0:T(8,128)}) %all-gather.17.cloned.1.call-update) | async-done | bytes 4227088 | tf_op jit(solution)/shard_map/all_gather | solution.py:30
  236.9 32.8 %all-to-all-done.1 = bf16[4,320,2048]{2,1,0:T(8,128)(2,1)} async-done(((bf16[4,320,2048]{2,1,0:T(8,128)(2,1)}), bf16[4,320,2048]{2,1,0:T(8,128)(2,1)}, u32[]{:S(2)}, u32[]{:S(2)}) %all-to-all-start.1) | async-done | bytes 5242912 | tf_op jit(solution)/shard_map/all_to_all | solution.py:61
  269.7 3.6 %reduce_sum.66 = bf16[320,2048]{1,0:T(8,128)(2,1)S(1)} reduce(bf16[4,320,2048]{2,1,0:T(8,128)(2,1)} %all-to-all-done.1, bf16[]{:T(256)} %constant.113.clone.1), dimensions={0}, to_apply=%region_11.12 | reduce | flops 1966080 | bytes 6553602 | tf_op jit(solution)/shard_map/reduce_sum | solution.py:62
  273.3 1.6 all_to_all.20
  275.0 10.7 %all-to-all-start.2 = ((bf16[64,5,2048]{2,1,0:T(8,128)(2,1)}), bf16[64,5,2048]{2,1,0:T(8,128)(2,1)S(1)}, u32[]{:S(2)}, u32[]{:S(2)}) async-start(bf16[64,5,2048]{2,1,0:T(8,128)(2,1)} %all_to_all.20), calls=%async_computation.2 | async-start | bytes 4194304 | tf_op jit(solution)/shard_map/all_to_all | solution.py:231
  286.5 2.8 fusion.130
  289.5 1.4 multiply_add_fusion.1
  291.1 1.5 fusion.20
  294.4 42.5 %all-to-all-done.2 = bf16[64,5,2048]{2,1,0:T(8,128)(2,1)S(1)} async-done(((bf16[64,5,2048]{2,1,0:T(8,128)(2,1)}), bf16[64,5,2048]{2,1,0:T(8,128)(2,1)S(1)}, u32[]{:S(2)}, u32[]{:S(2)}) %all-to-all-start.2) | async-done | bytes 1310752 | tf_op jit(solution)/shard_map/all_to_all | solution.py:231
  337.5 2.4 gather_fusion.1
  339.9 2.4 reshape.3367
  342.2 3.9 %multiply_reduce_fusion = bf16[128,2048]{1,0:T(8,128)(2,1)} fusion(f32[128,2,2048]{2,1,0:T(2,128)S(1)} %reshape.3367, f32[128,2]{1,0:T(8,128)S(1)} %copy.148), kind=kLoop, calls=%fused_computation.30 | loop fusion | flops 786432 | bytes 2622464 | tf_op jit(solution)/shard_map/reduce_sum | solution.py:233
  (273 shorter events, 43.8 us)
Async XLA Ops:
  7.2 42.7 %all-gather.13.cloned.1.call-start = ((), (), s32[]{:S(2)}) async-start(), calls=%async_computation.4 | async-start | bytes 1597440 | tf_op jit(solution)/shard_map/all_gather | solution.py:30
  32.4 88.8 %all-gather.15.cloned.1.call-start = ((), (), s32[]{:S(2)}) async-start(), calls=%async_computation.5 | async-start | bytes 2662400 | tf_op jit(solution)/shard_map/all_gather | solution.py:30
  54.4 122.3 %all-gather.11.cloned.1.call-start = ((), (), s32[]{:S(2)}) async-start(), calls=%async_computation.3 | async-start | bytes 6553600 | tf_op jit(solution)/shard_map/all_gather | solution.py:222
  121.0 113.3 %all-gather.17.cloned.1.call-start = ((), (), s32[]{:S(2)}) async-start(), calls=%async_computation.6 | async-start | bytes 4792320 | tf_op jit(solution)/shard_map/all_gather | solution.py:30
  204.4 65.3 %all-to-all-start.1 = ((bf16[4,320,2048]{2,1,0:T(8,128)(2,1)}), bf16[4,320,2048]{2,1,0:T(8,128)(2,1)}, u32[]{:S(2)}, u32[]{:S(2)}) async-start(bf16[4,320,2048]{2,1,0:T(8,128)(2,1)} %bitcast.529), calls=%async_computation.1 | async-start | bytes 10485760 | tf_op jit(solution)/shard_map/all_to_all | solution.py:61
  213.7 21.9 %copy-start.42 = (f32[2]{0:T(128)S(1)}, f32[2]{0:T(128)}, u32[]{:S(2)}) copy-start(f32[2]{0:T(128)} %copy-done.41) | copy-start | bytes 28
  213.7 21.9 %copy-start.44 = (f32[2]{0:T(128)S(1)}, f32[2]{0:T(128)}, u32[]{:S(2)}) copy-start(f32[2]{0:T(128)} %copy-done.43) | copy-start | bytes 28
  213.7 21.9 %copy-start.47 = (f32[2]{0:T(128)S(1)}, f32[2]{0:T(128)}, u32[]{:S(2)}) copy-start(f32[2]{0:T(128)} %copy-done.46) | copy-start | bytes 28
  213.7 21.9 %copy-start.49 = (f32[2]{0:T(128)S(1)}, f32[2]{0:T(128)}, u32[]{:S(2)}) copy-start(f32[2]{0:T(128)} %copy-done.48) | copy-start | bytes 28
  213.7 21.9 %copy-start.51 = (f32[2]{0:T(128)S(1)}, f32[2]{0:T(128)}, u32[]{:S(2)}) copy-start(f32[2]{0:T(128)} %copy-done.50) | copy-start | bytes 28
  213.7 21.9 %copy-start.53 = (f32[2]{0:T(128)S(1)}, f32[2]{0:T(128)}, u32[]{:S(2)}) copy-start(f32[2]{0:T(128)} %copy-done.52) | copy-start | bytes 28
  213.7 22.0 %copy-start.19 = (f32[2]{0:T(128)S(1)}, f32[2]{0:T(128)}, u32[]{:S(2)}) copy-start(f32[2]{0:T(128)} %copy-done.18) | copy-start | bytes 28
  213.8 22.0 %copy-start.21 = (f32[2]{0:T(128)S(1)}, f32[2]{0:T(128)}, u32[]{:S(2)}) copy-start(f32[2]{0:T(128)} %copy-done.20) | copy-start | bytes 28
  213.8 22.0 %copy-start.23 = (f32[2]{0:T(128)S(1)}, f32[2]{0:T(128)}, u32[]{:S(2)}) copy-start(f32[2]{0:T(128)} %copy-done.22) | copy-start | bytes 28
  213.8 22.0 %copy-start.25 = (f32[2]{0:T(128)S(1)}, f32[2]{0:T(128)}, u32[]{:S(2)}) copy-start(f32[2]{0:T(128)} %copy-done.24) | copy-start | bytes 28
  213.8 22.0 %copy-start.27 = (f32[2]{0:T(128)S(1)}, f32[2]{0:T(128)}, u32[]{:S(2)}) copy-start(f32[2]{0:T(128)} %copy-done.26) | copy-start | bytes 28
  213.8 22.0 %copy-start.29 = (f32[2]{0:T(128)S(1)}, f32[2]{0:T(128)}, u32[]{:S(2)}) copy-start(f32[2]{0:T(128)} %copy-done.28) | copy-start | bytes 28
  213.8 22.0 %copy-start.31 = (f32[2]{0:T(128)S(1)}, f32[2]{0:T(128)}, u32[]{:S(2)}) copy-start(f32[2]{0:T(128)} %copy-done.30) | copy-start | bytes 28
  213.8 22.0 %copy-start.33 = (f32[2]{0:T(128)S(1)}, f32[2]{0:T(128)}, u32[]{:S(2)}) copy-start(f32[2]{0:T(128)} %copy-done.32) | copy-start | bytes 28
  213.8 22.0 %copy-start.35 = (f32[2]{0:T(128)S(1)}, f32[2]{0:T(128)}, u32[]{:S(2)}) copy-start(f32[2]{0:T(128)} %copy-done.34) | copy-start | bytes 28
  213.8 22.0 %copy-start.37 = (f32[2]{0:T(128)S(1)}, f32[2]{0:T(128)}, u32[]{:S(2)}) copy-start(f32[2]{0:T(128)} %copy-done.36) | copy-start | bytes 28
  213.8 22.0 %copy-start.39 = (f32[2]{0:T(128)S(1)}, f32[2]{0:T(128)}, u32[]{:S(2)}) copy-start(f32[2]{0:T(128)} %copy-done.38) | copy-start | bytes 28
  213.9 23.0 %copy-start.45 = (f32[4,2,256]{2,1,0:T(2,128)S(1)}, f32[4,2,256]{2,1,0:T(2,128)}, u32[]{:S(2)}) copy-start(f32[4,2,256]{2,1,0:T(2,128)} %get-tuple-element.83) | copy-start | bytes 24580
  275.0 61.9 %all-to-all-start.2 = ((bf16[64,5,2048]{2,1,0:T(8,128)(2,1)}), bf16[64,5,2048]{2,1,0:T(8,128)(2,1)S(1)}, u32[]{:S(2)}, u32[]{:S(2)}) async-start(bf16[64,5,2048]{2,1,0:T(8,128)(2,1)} %all_to_all.20), calls=%async_computation.2 | async-start | bytes 4194304 | tf_op jit(solution)/shard_map/all_to_all | solution.py:231
  (41 other events, 213.5 us)
Sparse Core Ops, SparseCore 0:
  32.5 17.2 all-gather.12
  54.5 50.8 all-gather.14
  121.1 55.5 all-gather.10
  178.4 55.8 all-gather.16
where the time goes:
time: 354 us; the launch traced here: 353 us
  waiting for transfers between devices  160 us (45%)
  blocking collectives  61.6 us (17%)
  local copies, waits for them, and re-layouts  37.3 us (11%)
  matrix products  32.3 us (9%)
  other arithmetic  30.3 us (9%)
  starting transfers between devices  16.3 us (5%)
  between operations  15.1 us (4%)
    all_to_all x1, blocking collectives, local(): lax.all_to_all(sendbuf, EP, split_axis=0, concat_axis=0, tiled=True)  61.6 us
    all_gather x1, waiting for transfers between devices, local(): routed_rows = lax.all_gather(arrived, 'tp', axis=0, tiled=True)  49.9 us
    all_to_all x1, waiting for transfers between devices, local(): lax.all_to_all(summed, EP, split_axis=0, concat_axis=0, tiled=True)  42.5 us
    all_gather x3, waiting for transfers between devices, collected_together(): both, at, found = (lax.all_gather(jnp.concatenate(lines), axis), 0, {})  34.5 us
    all_to_all x1, waiting for transfers between devices, sum_at_owner(): blocks = lax.all_to_all(split_up(x, dim, size), axis, 0, 0, tiled=True)  32.8 us
    dot_general x1, matrix products, local(): jnp.dot(hidden, down_matrix, preferred_element_type=jnp.float32)  17.7 us
    all_to_all x1, starting transfers between devices, local(): lax.all_to_all(summed, EP, split_axis=0, concat_axis=0, tiled=True)  10.7 us
    dynamic_update_slice x8, local copies, waits for them, and re-layouts, mix_heads(): device_total, before = lax.scan(fold_step, identity_state, block_terms)  10.3 us
  transfers between devices with their start and end apart: 6, of which 5 were waited for; matrix products, arithmetic and copies ran while one was open for 15% of the time, Pallas kernels for 0%

commit v1 on v0

--- a/solution.py
+++ b/solution.py
@@ -219,7 +219,24 @@
         jnp.zeros((), jnp.bfloat16),
     )
     arrived = lax.all_to_all(sendbuf, EP, split_axis=0, concat_axis=0, tiled=True)
-    routed_rows = lax.all_gather(arrived, "tp", axis=0, tiled=True)
+    size_2, here_2, span = (lax.axis_size("tp"), lax.axis_index("tp"), arrived.shape[0])
+    right = [(i, (i + 1) % size_2) for i in range(size_2)]
+    behind = [(i, (i - 1) % size_2) for i in range(size_2)]
+    filled = jnp.zeros((*arrived.shape[:0], size_2 * span, *arrived.shape[0 + 1 :]), arrived.dtype)
+    filled = lax.dynamic_update_slice_in_dim(filled, arrived, here_2 * span, axis=0)
+    from_left = from_right = arrived
+    half = size_2 // 2
+    for step in range(1, half + 1):
+        from_left = lax.ppermute(from_left, "tp", right)
+        filled = lax.dynamic_update_slice_in_dim(
+            filled, from_left, (here_2 - step) % size_2 * span, axis=0
+        )
+        if step < size_2 - half:
+            from_right = lax.ppermute(from_right, "tp", behind)
+            filled = lax.dynamic_update_slice_in_dim(
+                filled, from_right, (here_2 + step) % size_2 * span, axis=0
+            )
+    routed_rows = filled
     gate_out = jnp.dot(routed_rows, gate_matrix, preferred_element_type=jnp.float32)
     up_out = jnp.dot(routed_rows, up_matrix, preferred_element_type=jnp.float32)
     hidden = (jax.nn.silu(gate_out) * up_out).astype(jnp.bfloat16)

time: 354 us -> 341 us (0.963)
  blocking collectives: 61.6 us -> 0 us
  waiting for transfers between devices: 160 us -> 179 us
  starting transfers between devices: 16.3 us -> 33.2 us
  local copies, waits for them, and re-layouts: 37.3 us -> 47 us
    all_to_all x1 -> x0, blocking collectives: 61.6 us -> none  [local(): lax.all_to_all(sendbuf, EP, split_axis=0, concat_axis=0, tiled=True)]
    all_gather x1 -> x0, waiting for transfers between devices: 49.9 us -> none  [local(): routed_rows = lax.all_gather(arrived, 'tp', axis=0, tiled=True)]
    all_to_all x0 -> x1, waiting for transfers between devices: none -> 46.5 us  [local(): lax.all_to_all(sendbuf, EP, split_axis=0, concat_axis=0, tiled=True)]
    ppermute x0 -> x3, waiting for transfers between devices: none -> 42.6 us  [the longest x2 42.6 us: local(): from_left = lax.ppermute(from_left, 'tp', right)]
    all_gather x3, waiting for transfers between devices: 34.5 us -> 0.04 us  [collected_together(): both, at, found = (lax.all_gather(jnp.concatenate(lines), axis), 0, {})]
    all_to_all x1, waiting for transfers between devices: 32.8 us -> 51.7 us  [sum_at_owner(): blocks = lax.all_to_all(split_up(x, dim, size), axis, 0, 0, tiled=True)]
    all_to_all x0 -> x1, starting transfers between devices: none -> 12.1 us  [local(): lax.all_to_all(sendbuf, EP, split_axis=0, concat_axis=0, tiled=True)]
    dynamic_update_slice x0 -> x4, local copies, waits for them, and re-layouts: none -> 7.51 us  [the longest x2 3.71 us: local(): lax.dynamic_update_slice_in_dim(filled, from_left, (here_2 - step) % size...]
  transfers between devices with their start and end apart: 6 -> 9, of which waited for: 5 -> 5; matrix products, arithmetic and copies ran while one was open for 15% -> 22% of each run, Pallas kernels for 0% -> 0%
where the time goes in v1:
time: 341 us; the launch traced here: 340 us
  waiting for transfers between devices  179 us (52%)
  local copies, waits for them, and re-layouts  47 us (14%)
  matrix products  34.3 us (10%)
  starting transfers between devices  33.2 us (10%)
  other arithmetic  31.6 us (9%)
  between operations  15 us (4%)
    all_to_all x1, waiting for transfers between devices, sum_at_owner(): blocks = lax.all_to_all(split_up(x, dim, size), axis, 0, 0, tiled=True)  51.7 us
    all_to_all x1, waiting for transfers between devices, local(): lax.all_to_all(sendbuf, EP, split_axis=0, concat_axis=0, tiled=True)  46.5 us
    ppermute x2, waiting for transfers between devices, local(): from_left = lax.ppermute(from_left, 'tp', right)  42.6 us
    all_to_all x1, waiting for transfers between devices, local(): lax.all_to_all(summed, EP, split_axis=0, concat_axis=0, tiled=True)  37.8 us
    dot_general x1, matrix products, local(): jnp.dot(hidden, down_matrix, preferred_element_type=jnp.float32)  17.6 us
    all_to_all x1, starting transfers between devices, local(): lax.all_to_all(summed, EP, split_axis=0, concat_axis=0, tiled=True)  12.2 us
    all_to_all x1, starting transfers between devices, local(): lax.all_to_all(sendbuf, EP, split_axis=0, concat_axis=0, tiled=True)  12.1 us
    dynamic_update_slice x8, local copies, waits for them, and re-layouts, mix_heads(): device_total, before = lax.scan(fold_step, identity_state, block_terms)  10.3 us
  transfers between devices with their start and end apart: 9, of which 5 were waited for; matrix products, arithmetic and copies ran while one was open for 22% of the time, Pallas kernels for 0%

profile of v1, /device:TPU:8, one launch (start us, length us, event | category | flops | bytes accessed | tf_op | source)
XLA Modules:
  0.0 340.1 jit_solution(7959544546572490662)
XLA Ops:
  12.4 2.0 fusion.41
  14.4 17.1 %while.25 = (s32[]{:T(128)}, f32[2,256,256]{2,1,0:T(8,128)S(1)}, f32[2,256]{1,0:T(2,128)S(1)}, f32[2]{0:T(128)S(1)}, f32[2]{0:T(128)S(1)}, /*index=5*/f32[4,2,25...) while((s32[]{:T(128)}, f32[2,256,256]{2,1,0:T(8,128)S(1)}, ...), condition=%wide.region_3.4_spmd.clone, body=%wide.region_2.3_spmd.clone.sunk | while | flops 657939 | bytes 2632044 | solution.py:120
  34.4 2.4 gather_fusion
  39.2 12.1 %all-to-all-start = ((bf16[64,5,2048]{2,1,0:T(8,128)(2,1)}), bf16[64,5,2048]{2,1,0:T(8,128)(2,1)S(1)}, u32[]{:S(2)}, u32[]{:S(2)}) async-start(bf16[64,5,2048]{2,1,0:T(8,128)(2,1)} %broadcast_select_fusion.3), calls=%async_computation | async-start | bytes 4194304 | tf_op jit(solution)/shard_map/all_to_all | solution.py:221
  56.0 46.5 %all-to-all-done = bf16[64,5,2048]{2,1,0:T(8,128)(2,1)S(1)} async-done(((bf16[64,5,2048]{2,1,0:T(8,128)(2,1)}), bf16[64,5,2048]{2,1,0:T(8,128)(2,1)S(1)}, u32[]{:S(2)}, u32[]{:S(2)}) %all-to-all-start) | async-done | bytes 1310752 | tf_op jit(solution)/shard_map/all_to_all | solution.py:221
  104.7 1.7 collective-permute-start.1
  106.4 3.1 broadcast_in_dim.54
  110.6 22.7 %collective-permute-done = bf16[320,2048]{1,0:T(8,128)(2,1)S(1)} collective-permute-done((bf16[320,2048]{1,0:T(8,128)(2,1)S(1)}, bf16[320,2048]{1,0:T(8,128)(2,1)S(1)}, u32[]{:S(2)}, u32[]{:S(2)}) %collective-permute-start) | collective-permute-done | bytes 1310752 | tf_op jit(solution)/shard_map/ppermute | solution.py:230
  134.8 2.6 constant_dynamic-update-slice_fusion.1
  140.0 2.0 fusion.30
  143.0 19.9 %collective-permute-done.2 = bf16[320,2048]{1,0:T(8,128)(2,1)} collective-permute-done((bf16[320,2048]{1,0:T(8,128)(2,1)S(1)}, bf16[320,2048]{1,0:T(8,128)(2,1)}, u32[]{:S(2)}, u32[]{:S(2)}) %collective-permute-start.2) | collective-permute-done | bytes 1310752 | tf_op jit(solution)/shard_map/ppermute | solution.py:230
  162.8 2.6 constant_dynamic-update-slice_fusion
  165.4 10.0 %fusion.14 = f32[1280,896]{1,0:T(8,128)} fusion(bf16[1280,2048]{1,0:T(8,128)(2,1)} %constant_dynamic-update-slice_fusion, bf16[1,2048,896]{2,1,0:T(8,128)(2,1)} %param.29), kind=kOutput, calls=%fused_computation.27 | convolution fusion | flops 4697620480 | bytes 13500416 | tf_op jit(solution)/shard_map/dot_general | solution.py:240
  175.4 17.6 %convolution_convert_fusion = bf16[1280,2048]{1,0:T(8,128)(2,1)} fusion(bf16[1,896,2048]{2,1,0:T(8,128)(2,1)} %param.31, f32[1280,896]{1,0:T(8,128)} %fusion.14, bf16[1280,2048]{1,0:T(8,128)(2,1)} %constant_dynamic-update-slice_fusion, bf16[1,2048,896]{2,1,0:T(8,128)(2,1)} %param.30), kind=kOutput, calls=%fused_computation.22 | convolution fusion | flops 9404743680 | bytes 22413312 | tf_op jit(solution)/shard_map/dot_general | solution.py:244
  193.0 5.2 %all-to-all-start.1 = ((bf16[4,320,2048]{2,1,0:T(8,128)(2,1)}), bf16[4,320,2048]{2,1,0:T(8,128)(2,1)}, u32[]{:S(2)}, u32[]{:S(2)}) async-start(bf16[4,320,2048]{2,1,0:T(8,128)(2,1)} %bitcast.531), calls=%async_computation.1 | async-start | bytes 10485760 | tf_op jit(solution)/shard_map/all_to_all | solution.py:61
  203.7 51.7 %all-to-all-done.1 = bf16[4,320,2048]{2,1,0:T(8,128)(2,1)} async-done(((bf16[4,320,2048]{2,1,0:T(8,128)(2,1)}), bf16[4,320,2048]{2,1,0:T(8,128)(2,1)}, u32[]{:S(2)}, u32[]{:S(2)}) %all-to-all-start.1) | async-done | bytes 5242912 | tf_op jit(solution)/shard_map/all_to_all | solution.py:61
  255.4 3.6 %reduce_sum.66 = bf16[320,2048]{1,0:T(8,128)(2,1)S(1)} reduce(bf16[4,320,2048]{2,1,0:T(8,128)(2,1)} %all-to-all-done.1, bf16[]{:T(256)} %constant.134.clone.1), dimensions={0}, to_apply=%region_11.12 | reduce | flops 1966080 | bytes 6553602 | tf_op jit(solution)/shard_map/reduce_sum | solution.py:62
  259.0 1.6 all_to_all.20
  260.8 12.2 %all-to-all-start.2 = ((bf16[64,5,2048]{2,1,0:T(8,128)(2,1)}), bf16[64,5,2048]{2,1,0:T(8,128)(2,1)S(1)}, u32[]{:S(2)}, u32[]{:S(2)}) async-start(bf16[64,5,2048]{2,1,0:T(8,128)(2,1)} %all_to_all.20), calls=%async_computation.2 | async-start | bytes 4194304 | tf_op jit(solution)/shard_map/all_to_all | solution.py:248
  278.5 2.8 fusion.133
  286.4 37.8 %all-to-all-done.2 = bf16[64,5,2048]{2,1,0:T(8,128)(2,1)S(1)} async-done(((bf16[64,5,2048]{2,1,0:T(8,128)(2,1)}), bf16[64,5,2048]{2,1,0:T(8,128)(2,1)S(1)}, u32[]{:S(2)}, u32[]{:S(2)}) %all-to-all-start.2) | async-done | bytes 1310752 | tf_op jit(solution)/shard_map/all_to_all | solution.py:248
  324.9 2.4 gather_fusion.1
  327.2 2.4 reshape.3367
  329.6 3.9 %multiply_reduce_fusion = bf16[128,2048]{1,0:T(8,128)(2,1)} fusion(f32[128,2,2048]{2,1,0:T(2,128)S(1)} %reshape.3367, f32[128,2]{1,0:T(8,128)S(1)} %copy.148), kind=kLoop, calls=%fused_computation.31 | loop fusion | flops 786432 | bytes 2622464 | tf_op jit(solution)/shard_map/reduce_sum | solution.py:250
  (280 shorter events, 56.1 us)
Async XLA Ops:
  7.2 44.2 %all-gather.10.cloned.1.call-start = ((), (), s32[]{:S(2)}) async-start(), calls=%async_computation.3 | async-start | bytes 1597440 | tf_op jit(solution)/shard_map/all_gather | solution.py:30
  14.4 18.0 %copy-start.53 = (s32[128,2]{0,1:T(2,128)S(1)}, s32[128,2]{0,1:T(2,128)}, u32[]{:S(2)}) copy-start(s32[128,2]{0,1:T(2,128)} %param.27) | copy-start | bytes 3076
  39.2 63.3 %all-to-all-start = ((bf16[64,5,2048]{2,1,0:T(8,128)(2,1)}), bf16[64,5,2048]{2,1,0:T(8,128)(2,1)S(1)}, u32[]{:S(2)}, u32[]{:S(2)}) async-start(bf16[64,5,2048]{2,1,0:T(8,128)(2,1)} %broadcast_select_fusion.3), calls=%async_computation | async-start | bytes 4194304 | tf_op jit(solution)/shard_map/all_to_all | solution.py:221
  51.3 86.2 %all-gather.12.cloned.1.call-start = ((), (), s32[]{:S(2)}) async-start(), calls=%async_computation.4 | async-start | bytes 2662400 | tf_op jit(solution)/shard_map/all_gather | solution.py:30
  52.2 50.9 %copy-start.31 = (f32[2]{0:T(128)}, f32[2]{0:T(128)S(1)}, u32[]{:S(2)}) copy-start(f32[2]{0:T(128)S(1)} %get-tuple-element.244) | copy-start | bytes 28
  52.2 50.8 %copy-start.33 = (f32[2]{0:T(128)}, f32[2]{0:T(128)S(1)}, u32[]{:S(2)}) copy-start(f32[2]{0:T(128)S(1)} %get-tuple-element.299) | copy-start | bytes 28
  55.9 217.1 %all-gather.14.cloned.1.call-start = ((), (), s32[]{:S(2)}) async-start(), calls=%async_computation.5 | async-start | bytes 4792320 | tf_op jit(solution)/shard_map/all_gather | solution.py:30
  103.1 30.3 %collective-permute-start = (bf16[320,2048]{1,0:T(8,128)(2,1)S(1)}, bf16[320,2048]{1,0:T(8,128)(2,1)S(1)}, u32[]{:S(2)}, u32[]{:S(2)}) collective-permute-start(bf16[320,2048]{1,0:T(8,128)(2,1)S(1)} %all_to_all.18), channel_id=1, source_target_pairs={{0,1},{1,2},{2,3},{3,0},{4,5},{5,6},{6,7},{7,4},{8,9},{9,10},{10,1... | collective-permute-start | bytes 3932168 | tf_op jit(solution)/shard_map/ppermute | solution.py:230
  104.7 30.1 %collective-permute-start.1 = (bf16[320,2048]{1,0:T(8,128)(2,1)S(1)}, bf16[320,2048]{1,0:T(8,128)(2,1)}, u32[]{:S(2)}, u32[]{:S(2)}) collective-permute-start(bf16[320,2048]{1,0:T(8,128)(2,1)S(1)} %all_to_all.18), channel_id=1, source_target_pairs={{0,3},{1,0},{2,1},{3,2},{4,7},{5,4},{6,5},{7,6},{8,11},{9,8},{10,9... | collective-permute-start | bytes 3932168 | tf_op jit(solution)/shard_map/ppermute | solution.py:235
  133.4 29.5 %collective-permute-start.2 = (bf16[320,2048]{1,0:T(8,128)(2,1)S(1)}, bf16[320,2048]{1,0:T(8,128)(2,1)}, u32[]{:S(2)}, u32[]{:S(2)}) collective-permute-start(bf16[320,2048]{1,0:T(8,128)(2,1)S(1)} %collective-permute-done), channel_id=1, source_target_pairs={{0,1},{1,2},{2,3},{3,0},{4,5},{5,6},{6,7},{7,4},{8,9},{9,10},{10,1... | collective-permute-start | bytes 3932168 | tf_op jit(solution)/shard_map/ppermute | solution.py:230
  193.0 62.3 %all-to-all-start.1 = ((bf16[4,320,2048]{2,1,0:T(8,128)(2,1)}), bf16[4,320,2048]{2,1,0:T(8,128)(2,1)}, u32[]{:S(2)}, u32[]{:S(2)}) async-start(bf16[4,320,2048]{2,1,0:T(8,128)(2,1)} %bitcast.531), calls=%async_computation.1 | async-start | bytes 10485760 | tf_op jit(solution)/shard_map/all_to_all | solution.py:61
  260.7 13.8 %copy-start.18 = (f32[2]{0:T(128)S(1)}, f32[2]{0:T(128)}, u32[]{:S(2)}) copy-start(f32[2]{0:T(128)} %copy-done.17) | copy-start | bytes 28
  260.7 13.8 %copy-start.20 = (f32[2]{0:T(128)S(1)}, f32[2]{0:T(128)}, u32[]{:S(2)}) copy-start(f32[2]{0:T(128)} %copy-done.19) | copy-start | bytes 28
  260.7 13.8 %copy-start.22 = (f32[2]{0:T(128)S(1)}, f32[2]{0:T(128)}, u32[]{:S(2)}) copy-start(f32[2]{0:T(128)} %copy-done.21) | copy-start | bytes 28
  260.7 13.8 %copy-start.24 = (f32[2]{0:T(128)S(1)}, f32[2]{0:T(128)}, u32[]{:S(2)}) copy-start(f32[2]{0:T(128)} %copy-done.23) | copy-start | bytes 28
  260.7 13.8 %copy-start.26 = (f32[2]{0:T(128)S(1)}, f32[2]{0:T(128)}, u32[]{:S(2)}) copy-start(f32[2]{0:T(128)} %copy-done.25) | copy-start | bytes 28
  260.7 13.8 %copy-start.28 = (f32[2]{0:T(128)S(1)}, f32[2]{0:T(128)}, u32[]{:S(2)}) copy-start(f32[2]{0:T(128)} %copy-done.27) | copy-start | bytes 28
  260.8 13.8 %copy-start.30 = (f32[2]{0:T(128)S(1)}, f32[2]{0:T(128)}, u32[]{:S(2)}) copy-start(f32[2]{0:T(128)} %copy-done.29) | copy-start | bytes 28
  260.8 13.8 %copy-start.32 = (f32[2]{0:T(128)S(1)}, f32[2]{0:T(128)}, u32[]{:S(2)}) copy-start(f32[2]{0:T(128)} %copy-done.31) | copy-start | bytes 28
  260.8 13.8 %copy-start.34 = (f32[2]{0:T(128)S(1)}, f32[2]{0:T(128)}, u32[]{:S(2)}) copy-start(f32[2]{0:T(128)} %copy-done.33) | copy-start | bytes 28
  260.8 13.8 %copy-start.36 = (f32[2]{0:T(128)S(1)}, f32[2]{0:T(128)}, u32[]{:S(2)}) copy-start(f32[2]{0:T(128)} %copy-done.35) | copy-start | bytes 28
  260.8 13.8 %copy-start.38 = (f32[2]{0:T(128)S(1)}, f32[2]{0:T(128)}, u32[]{:S(2)}) copy-start(f32[2]{0:T(128)} %copy-done.37) | copy-start | bytes 28
  260.8 14.8 %copy-start.44 = (f32[4,2,256]{2,1,0:T(2,128)S(1)}, f32[4,2,256]{2,1,0:T(2,128)}, u32[]{:S(2)}) copy-start(f32[4,2,256]{2,1,0:T(2,128)} %get-tuple-element.83) | copy-start | bytes 24580
  260.8 63.5 %all-to-all-start.2 = ((bf16[64,5,2048]{2,1,0:T(8,128)(2,1)}), bf16[64,5,2048]{2,1,0:T(8,128)(2,1)S(1)}, u32[]{:S(2)}, u32[]{:S(2)}) async-start(bf16[64,5,2048]{2,1,0:T(8,128)(2,1)} %all_to_all.20), calls=%async_computation.2 | async-start | bytes 4194304 | tf_op jit(solution)/shard_map/all_to_all | solution.py:248
  (43 other events, 231.7 us)
Sparse Core Ops, SparseCore 0:
  32.5 17.2 all-gather.9
  56.1 46.2 all-gather.11
  143.0 53.0 all-gather.13
